TPU v7x, 128 devices: a whole 4x4x4 slice. The times are simulated.
128 devices in a mesh: ep: 64 (over z, y, x), tp: 2 (over core).
Axes of the slice: x: 4, y: 4, z: 4, core: 2. Of those that a mesh axis runs over, the one named last changes fastest.
Arguments:
- tokens: bfloat16 [2048, 3072], P('ep'), may hold values from -6 to 6
- carried: float32 [2048, 96, 128], P('ep', 'tp'), may hold values from -4 to 4
- decay_rate: float32 [96, 64], P('tp'), may hold values from 0.02 to 20
- frequency: float32 [96, 64], P('tp'), may hold values from 0 to 200
- log_step: float32 [96], P('tp'), may hold values from -4.6 to 0
- in_map: bfloat16 [96, 128, 16], P('tp'), may hold values from -1 to 1
- out_map: bfloat16 [96, 16, 128], P('tp'), may hold values from -0.5 to 0.5
- skip_gain: float32 [1536], P('tp'), may hold values from -4 to 4
- norm_gain: float32 [3072], replicated, may hold values from 0.1 to 1.9
- w_in: bfloat16 [3072, 1536], P(None, 'tp'), may hold values from -0.109375 to 0.109375
- w_out: bfloat16 [1536, 3072], P('tp'), may hold values from -0.15625 to 0.15625
- expert_gain: float32 [3072], replicated, may hold values from 0.1 to 1.9
- route_ids: int32 [2048, 2], P('ep'), may hold values from 0 to 7, all different within a row; in each aligned block of 32 rows (0 to 31, 32 to 63, ...) at most 16 rows name the same one
- route_logit: float32 [2048, 2], P('ep'), may hold values from -6 to 6
- w_gate: bfloat16 [3072, 43008], P(None, ('ep', 'tp')), may hold values from -0.109375 to 0.109375
- w_up: bfloat16 [3072, 43008], P(None, ('ep', 'tp')), may hold values from -0.109375 to 0.109375
- w_down: bfloat16 [43008, 3072], P(('ep', 'tp')), may hold values from -0.078125 to 0.078125
Outputs:
- new_tokens: bfloat16 [2048, 3072], P('ep', 'tp')
- new_carried: float32 [2048, 96, 128], P('ep', 'tp')
Inputs may be any that keep to these rules, and one draw needn't show every extreme that they name: `route_ids`: each row names 2 different experts; within each aligned block of 32 rows (the rows of one index of ep) no expert is named by more than 16 rows, a bound that some block reaches.
All inputs are finite; a program needn't handle non-finite values.
Results may differ from a plain program's by a relative error of at most 0.014.
Values may be sent and summed in bfloat16 or wider, within the bound.
No kernel may reach another device: no remote copies, remote signals or barrier semaphores. Data moves between devices by JAX's collectives and lax.ppermute only.
A program may use at most 128 MiB of HBM per device.

v0:
```python
import jax
import jax.numpy as jnp
from jax import lax
from jax.sharding import PartitionSpec as P

EXPERTS = 8
TOP = 2
CAP = 16


def copy_for_each(shard, axis):
    copies = jnp.broadcast_to(shard, (lax.axis_size(axis), *shard.shape))
    return lax.all_to_all(copies, axis, split_axis=0, concat_axis=0, tiled=True)


def taken_together(shard, axis):
    return copy_for_each(shard, axis).astype(jnp.float32).sum(axis=0)


def normalize(rows, gain):
    wide = rows.astype(jnp.float32)
    scaled = wide * lax.rsqrt(jnp.mean(wide * wide, axis=-1, keepdims=True) + 1e-06)
    return (scaled * gain).astype(jnp.bfloat16)


def state_update(drive, carried, decay_rate, frequency, log_step, in_map, out_map, skip_gain):
    count_rows, width = drive.shape
    groups, half = decay_rate.shape
    channels = width // groups
    step_size = jnp.exp(log_step)[:, None]
    magnitude = jnp.exp(-decay_rate * step_size)
    real_decay = magnitude * jnp.cos(frequency * step_size)
    imag_decay = magnitude * jnp.sin(frequency * step_size)
    denom = decay_rate * decay_rate + frequency * frequency
    real_less = real_decay - 1.0
    real_factor = (-real_less * decay_rate + imag_decay * frequency) / denom
    imag_factor = (-imag_decay * decay_rate - real_less * frequency) / denom
    grouped_drive = drive.reshape(count_rows, groups, channels)
    projected = jnp.einsum(
        "sgh,gqh->sgq", grouped_drive, in_map, preferred_element_type=jnp.float32
    )
    real_in = projected[..., :half]
    imag_in = projected[..., half:]
    real_push = real_factor * real_in - imag_factor * imag_in
    imag_push = real_factor * imag_in + imag_factor * real_in
    real_old = carried[..., :half]
    imag_old = carried[..., half:]
    real_new = real_decay * real_old - imag_decay * imag_old + real_push
    imag_new = real_decay * imag_old + imag_decay * real_old + imag_push
    joined = jnp.concatenate([real_new, -imag_new], axis=-1)
    reading = jnp.einsum("sgq,ghq->sgh", joined, out_map.astype(jnp.float32))
    total = reading.reshape(count_rows, width) + skip_gain * drive.astype(jnp.float32)
    activated = jax.nn.gelu(total).astype(jnp.bfloat16)
    return (activated, jnp.concatenate([real_new, imag_new], axis=-1))


def route_weights(route_logit):
    first = jax.nn.sigmoid(route_logit[:, 0] - route_logit[:, 1])
    second = jax.nn.sigmoid(route_logit[:, 1] - route_logit[:, 0])
    return jnp.stack([first, second], axis=1)


def per_device(
    tokens,
    carried,
    decay_rate,
    frequency,
    log_step,
    in_map,
    out_map,
    skip_gain,
    norm_gain,
    w_in,
    w_out,
    expert_gain,
    route_ids,
    route_logit,
    w_gate,
    w_up,
    w_down,
):
    count_rows, model_width = tokens.shape
    normed = normalize(tokens, norm_gain)
    drive = jnp.dot(normed, w_in, preferred_element_type=jnp.float32).astype(jnp.bfloat16)
    activated, new_carried = state_update(
        drive, carried, decay_rate, frequency, log_step, in_map, out_map, skip_gain
    )
    partial_value = jnp.dot(activated, w_out, preferred_element_type=jnp.float32).astype(
        jnp.bfloat16
    )
    summed = taken_together(partial_value.astype(jnp.float32).astype(jnp.bfloat16), "tp").astype(
        jnp.float32
    )
    mixed = (tokens.astype(jnp.float32) + summed).astype(jnp.bfloat16)
    expert_in = normalize(mixed, expert_gain)
    weights = route_weights(route_logit)
    ep_count = lax.axis_size("ep")
    group_size = ep_count // EXPERTS
    expert_ids = jnp.arange(EXPERTS, dtype=jnp.int32)
    routes_flat = route_ids.reshape(-1)
    weights_flat = weights.reshape(-1)
    onehot = (routes_flat[:, None] == expert_ids[None, :]).astype(jnp.int32)
    earlier = jnp.cumsum(onehot, axis=0) - onehot
    slot_index = jnp.sum(earlier * onehot, axis=1)
    position = routes_flat * CAP + slot_index
    placement = (jnp.arange(EXPERTS * CAP, dtype=jnp.int32)[:, None] == position[None, :]).astype(
        jnp.float32
    )
    per_token = placement.reshape(EXPERTS * CAP, count_rows, TOP).sum(axis=2)
    packed = jnp.dot(per_token.astype(jnp.bfloat16), expert_in, preferred_element_type=jnp.float32)
    packed = packed.astype(jnp.bfloat16).reshape(EXPERTS, CAP, model_width)
    outgoing = jnp.repeat(packed, group_size, axis=0)
    received = lax.all_to_all(outgoing, "ep", split_axis=0, concat_axis=0, tiled=True)
    sources, slots, features = received.shape
    rows = received.reshape(sources * slots, features)
    gated = jnp.dot(rows, w_gate, preferred_element_type=jnp.float32)
    upward = jnp.dot(rows, w_up, preferred_element_type=jnp.float32)
    hidden = (jax.nn.silu(gated) * upward).astype(jnp.bfloat16)
    produced = jnp.dot(hidden, w_down, preferred_element_type=jnp.float32)
    produced = produced.reshape(sources, slots, features)
    halves = lax.psum_scatter(
        produced.astype(jnp.bfloat16), "tp", scatter_dimension=2, tiled=True
    ).astype(jnp.float32)
    returned = lax.all_to_all(
        halves.astype(jnp.bfloat16), "ep", split_axis=0, concat_axis=0, tiled=True
    ).astype(halves.dtype)
    per_expert = returned.reshape(EXPERTS, group_size, CAP, -1).sum(axis=1)
    per_expert = per_expert.reshape(EXPERTS * CAP, -1)
    weighing = (
        (placement * weights_flat[None, :]).reshape(EXPERTS * CAP, count_rows, TOP).sum(axis=2)
    )
    expert_sum = jnp.dot(weighing.T, per_expert, preferred_element_type=jnp.float32)
    half_width = model_width // lax.axis_size("tp")
    column_start = lax.axis_index("tp") * half_width
    own_mixed = lax.dynamic_slice_in_dim(mixed, column_start, half_width, 1)
    new_tokens = (own_mixed.astype(jnp.float32) + expert_sum).astype(jnp.bfloat16)
    return (new_tokens, new_carried)


def solution(mesh):
    return jax.shard_map(
        per_device,
        mesh=mesh,
        in_specs=(
            P("ep", None),
            P("ep", "tp", None),
            P("tp", None),
            P("tp", None),
            P("tp"),
            P("tp", None, None),
            P("tp", None, None),
            P("tp"),
            P(),
            P(None, "tp"),
            P("tp", None),
            P(),
            P("ep", None),
            P("ep", None),
            P(None, ("ep", "tp")),
            P(None, ("ep", "tp")),
            P(("ep", "tp"), None),
        ),
        out_specs=(P("ep", "tp"), P("ep", "tp", None)),
        check_vma=False,
    )
```

profile of v0, /device:TPU:0, one launch (start us, length us, event | category | flops | bytes accessed | tf_op | source)
XLA Modules:
  0.0 208.2 jit_solution(8100006925900733602)
XLA Ops:
  7.2 0.0 copy-start
  7.2 0.8 exp.18
  8.0 1.1 fusion.9
  9.1 0.0 copy-start.2
  9.1 3.5 %convolution_convert_fusion.3 = bf16[32,768]{1,0:T(8,128)(2,1)S(1)} fusion(bf16[3072,768]{1,0:T(8,128)(2,1)} %param.26, bf16[32,3072]{1,0:T(8,128)(2,1)} %param.17, f32[3072]{0:T(1024)} %param.25, f32[32]{0:T(128)S(1)} %add_rsqrt_fusion.1), kind=kOutput, calls=%fused_computation.9 | convolution fusion | flops 151412736 | bytes 4976768 | tf_op jit(solution)/shard_map/dot_general | solution.py:84
  12.6 0.0 copy-start.4
  12.6 0.2 copy.48
  12.8 0.0 copy-start.6
  12.8 0.0 copy-start.7
  12.8 0.3 fusion.44
  13.0 0.5 copy-done.4
  13.5 0.3 convolution_bitcast_fusion
  13.9 0.2 cosine_multiply_fusion
  14.0 0.7 subtract_add_fusion
  14.8 1.6 fusion.43
  16.4 0.4 fusion.2
  16.8 0.1 copy.49
  17.0 0.1 copy-done.10
  17.1 3.2 %convolution_convert_fusion.2 = bf16[32,3072]{1,0:T(8,128)(2,1)S(1)} fusion(bf16[768,3072]{1,0:T(8,128)(2,1)} %param.27, f32[32,768]{1,0:T(8,128)S(1)} %copy.49, bf16[32,768]{1,0:T(8,128)(2,1)S(1)} %convolution_convert_fusion.3, f32[768]{0:T(1024)S(1)} %copy-done.10), kind=kOutput, calls=%fused_computation.3 | convolution fusion | flops 151388160 | bytes 5065728 | tf_op jit(solution)/shard_map/dot_general | solution.py:88
  20.3 0.0 copy-start.8
  20.4 0.8 broadcast_in_dim.4
  21.1 3.5 %all-to-all-start = ((bf16[2,32,3072]{2,1,0:T(8,128)(2,1)}), bf16[2,32,3072]{2,1,0:T(8,128)(2,1)S(1)}, u32[]{:S(2)}, u32[]{:S(2)}) async-start(bf16[2,32,3072]{2,1,0:T(8,128)(2,1)} %broadcast_in_dim.4), calls=%async_computation | async-start | bytes 786432 | tf_op jit(solution)/shard_map/all_to_all | solution.py:13
  24.6 0.0 reduce-scatter.2.cloned.1.call-start
  24.7 0.1 copy.50
  24.8 0.1 eq.31
  24.9 0.1 fusion.33
  25.0 0.1 reduce_window_sum.11
  25.1 0.2 select_reduce_fusion.1
  25.2 0.1 reduce_sum.68
  25.4 0.1 copy.51
  25.4 0.8 all-to-all-done
  26.2 0.1 convert_reduce_fusion.1
  26.3 0.2 fusion.6
  26.5 0.1 convert_reduce_fusion.2
  26.6 0.4 convolution_convert_fusion.1
  27.0 0.8 broadcast_in_dim.5
  27.8 86.8 %all_to_all.15 = bf16[64,16,3072]{2,1,0:T(8,128)(2,1)S(1)} all-to-all(bf16[64,16,3072]{2,1,0:T(8,128)(2,1)S(1)} %bitcast.27), channel_id=1, replica_groups=mesh['ep'=64,'tp'=2] {'ep'}, dimensions={0} | all-to-all | bytes 12582912 | tf_op jit(solution)/shard_map/all_to_all | solution.py:113
  114.7 2.7 %copy-done.1 = bf16[64,16,3072]{2,1,0:T(8,128)(2,1)} copy-done((bf16[64,16,3072]{2,1,0:T(8,128)(2,1)}, bf16[64,16,3072]{2,1,0:T(8,128)(2,1)S(1)}, u32[]{:S(2)}) %copy-start.1) | copy-done | bytes 6291480
  117.3 3.5 %fusion.45 = f32[1024,336]{0,1:T(8,128)} fusion(bf16[1024,3072]{1,0:T(8,128)(2,1)S(1)} %bitcast.29, bf16[3072,336]{0,1:T(8,128)(2,1)S(1)} %copy-done.12), kind=kOutput, calls=%fused_computation.75 | convolution fusion | flops 2113929216 | bytes 9732096 | tf_op jit(solution)/shard_map/dot_general | solution.py:116
  120.8 10.6 %convolution_convert_fusion = bf16[1024,3072]{1,0:T(8,128)(2,1)} fusion(bf16[336,3072]{1,0:T(8,128)(2,1)S(1)} %copy-done, bf16[1024,3072]{1,0:T(8,128)(2,1)} %bitcast.30, bf16[3072,336]{0,1:T(8,128)(2,1)} %param.32, f32[1024,336]{0,1:T(8,128)} %fusion.45), kind=kOutput, calls=%fused_computation.1 | convolution fusion | flops 4233068544 | bytes 18087936 | tf_op jit(solution)/shard_map/dot_general | solution.py:119
  131.4 0.0 reduce-scatter.2.cloned.1.call-update
  131.5 13.6 %reduce-scatter.2.cloned.1.call-done = bf16[64,16,1536]{2,1,0:T(8,128)(2,1)} async-done(((bf16[64,16,3072]{2,1,0:T(8,128)(2,1)}), bf16[64,16,1536]{2,1,0:T(8,128)(2,1)}) %reduce-scatter.2.cloned.1.call-update) | async-done | bytes 3145744 | tf_op jit(solution)/shard_map/reduce_scatter | solution.py:121
  145.1 10.6 %all-to-all-start.2 = ((bf16[64,16,1536]{2,1,0:T(8,128)(2,1)}), bf16[64,16,1536]{2,1,0:T(8,128)(2,1)}, u32[]{:S(2)}, u32[]{:S(2)}) async-start(bf16[64,16,1536]{2,1,0:T(8,128)(2,1)} %reduce-scatter.2.cloned.1.call-done), calls=%async_computation.3 | async-start | bytes 6291456 | tf_op jit(solution)/shard_map/all_to_all | solution.py:124
  155.7 1.4 pad_maximum_fusion
  157.1 1.3 copy.52
  158.5 39.6 %all-to-all-done.2 = bf16[64,16,1536]{2,1,0:T(8,128)(2,1)} async-done(((bf16[64,16,1536]{2,1,0:T(8,128)(2,1)}), bf16[64,16,1536]{2,1,0:T(8,128)(2,1)}, u32[]{:S(2)}, u32[]{:S(2)}) %all-to-all-start.2) | async-done | bytes 3145760 | tf_op jit(solution)/shard_map/all_to_all | solution.py:124
  198.1 2.4 %convert_reduce_fusion = bf16[8,16,1536]{2,1,0:T(8,128)(2,1)S(1)} fusion(bf16[64,16,1536]{2,1,0:T(8,128)(2,1)} %all-to-all-done.2), kind=kLoop, calls=%fused_computation | loop fusion | flops 2949120 | bytes 3538944 | tf_op jit(solution)/shard_map/reduce_sum | solution.py:127
  200.5 0.8 fusion
  (22 shorter events, 0.1 us)
Async XLA Ops:
  7.2 113.6 %copy-start = (bf16[336,3072]{1,0:T(8,128)(2,1)S(1)}, bf16[336,3072]{1,0:T(8,128)(2,1)}, u32[]{:S(2)}) copy-start(bf16[336,3072]{1,0:T(8,128)(2,1)} %param.33) | copy-start | bytes 6193156
  9.1 3.7 %copy-start.2 = (f32[32,48,128]{2,1,0:T(8,128)S(1)}, f32[32,48,128]{2,1,0:T(8,128)}, u32[]{:S(2)}) copy-start(f32[32,48,128]{2,1,0:T(8,128)} %param.18) | copy-start | bytes 2359300
  12.6 0.9 copy-start.4
  12.8 1.1 copy-start.6
  12.8 1.1 copy-start.7
  14.8 1.6 copy-start.5
  16.4 0.7 copy-start.10
  17.1 7.6 %copy-start.11 = (f32[32,2]{0,1:T(2,128)S(1)}, f32[32,2]{0,1:T(2,128)}, u32[]{:S(2)}) copy-start(f32[32,2]{0,1:T(2,128)} %param.30) | copy-start | bytes 772
  17.1 7.6 %copy-start.9 = (s32[32,2]{0,1:T(2,128)S(1)}, s32[32,2]{0,1:T(2,128)}, u32[]{:S(2)}) copy-start(s32[32,2]{0,1:T(2,128)} %param.29) | copy-start | bytes 772
  20.3 6.0 %copy-start.3 = (bf16[32,3072]{1,0:T(8,128)(2,1)S(1)}, bf16[32,3072]{1,0:T(8,128)(2,1)}, u32[]{:S(2)}) copy-start(bf16[32,3072]{1,0:T(8,128)(2,1)} %param.17) | copy-start | bytes 589828
  20.3 6.3 %copy-start.8 = (f32[3072]{0:T(1024)S(1)}, f32[3072]{0:T(1024)}, u32[]{:S(2)}) copy-start(f32[3072]{0:T(1024)} %param.28) | copy-start | bytes 36868
  21.1 5.1 %all-to-all-start = ((bf16[2,32,3072]{2,1,0:T(8,128)(2,1)}), bf16[2,32,3072]{2,1,0:T(8,128)(2,1)S(1)}, u32[]{:S(2)}, u32[]{:S(2)}) async-start(bf16[2,32,3072]{2,1,0:T(8,128)(2,1)} %broadcast_in_dim.4), calls=%async_computation | async-start | bytes 786432 | tf_op jit(solution)/shard_map/all_to_all | solution.py:13
  24.6 120.5 %reduce-scatter.2.cloned.1.call-start = ((), (), s32[]{:S(2)}) async-start(), calls=%async_computation.4 | async-start | bytes 9437184 | tf_op jit(solution)/shard_map/reduce_scatter | solution.py:121
  27.8 89.5 %copy-start.12 = (bf16[3072,336]{0,1:T(8,128)(2,1)S(1)}, bf16[3072,336]{0,1:T(8,128)(2,1)}, u32[]{:S(2)}) copy-start(bf16[3072,336]{0,1:T(8,128)(2,1)} %param.31) | copy-start | bytes 6193156
  114.7 2.7 %copy-start.1 = (bf16[64,16,3072]{2,1,0:T(8,128)(2,1)}, bf16[64,16,3072]{2,1,0:T(8,128)(2,1)S(1)}, u32[]{:S(2)}) copy-start(bf16[64,16,3072]{2,1,0:T(8,128)(2,1)S(1)} %all_to_all.15) | copy-start | bytes 18874372
  145.1 53.0 %all-to-all-start.2 = ((bf16[64,16,1536]{2,1,0:T(8,128)(2,1)}), bf16[64,16,1536]{2,1,0:T(8,128)(2,1)}, u32[]{:S(2)}, u32[]{:S(2)}) async-start(bf16[64,16,1536]{2,1,0:T(8,128)(2,1)} %reduce-scatter.2.cloned.1.call-done), calls=%async_computation.3 | async-start | bytes 6291456 | tf_op jit(solution)/shard_map/all_to_all | solution.py:124
Sparse Core Ops, SparseCore 0:
  131.6 13.4 reduce-scatter.1
where the time goes:
time: 209 us; the launch traced here: 208 us
  blocking collectives  86.8 us (42%)
  waiting for transfers between devices  54.1 us (26%)
  matrix products  22.8 us (11%)
  between operations  14.3 us (7%)
  starting transfers between devices  14.1 us (7%)
  other arithmetic  8.11 us (4%)
  local copies, waits for them, and re-layouts  7.96 us (4%)
    all_to_all x1, blocking collectives, per_device(): lax.all_to_all(outgoing, 'ep', split_axis=0, concat_axis=0, tiled=True)  86.8 us
    all_to_all x1, waiting for transfers between devices, per_device(): lax.all_to_all(halves.astype(jnp.bfloat16), 'ep', split_axis=0, concat_ax...  39.6 us
    reduce_scatter x1, waiting for transfers between devices, per_device(): lax.psum_scatter(produced.astype(jnp.bfloat16), 'tp', scatter_dimension=2...  13.6 us
    dot_general x1, matrix products, per_device(): produced = jnp.dot(hidden, w_down, preferred_element_type=jnp.float32)  10.6 us
    all_to_all x1, starting transfers between devices, per_device(): lax.all_to_all(halves.astype(jnp.bfloat16), 'ep', split_axis=0, concat_ax...  10.6 us
    unnamed x28, local copies, waits for them, and re-layouts  4.75 us
  transfers between devices with their start and end apart: 3, of which 3 were waited for; matrix products, arithmetic and copies ran while one was open for 2% of the time, Pallas kernels for 0%

commit v1 on v0

--- a/solution.py
+++ b/solution.py
@@ -8,13 +8,8 @@
 CAP = 16
 
 
-def copy_for_each(shard, axis):
-    copies = jnp.broadcast_to(shard, (lax.axis_size(axis), *shard.shape))
-    return lax.all_to_all(copies, axis, split_axis=0, concat_axis=0, tiled=True)
-
-
-def taken_together(shard, axis):
-    return copy_for_each(shard, axis).astype(jnp.float32).sum(axis=0)
+def swapped(shard):
+    return lax.ppermute(shard, "tp", [(0, 1), (1, 0)])
 
 
 def normalize(rows, gain):
@@ -80,6 +75,9 @@
     w_down,
 ):
     count_rows, model_width = tokens.shape
+    core = lax.axis_index("tp")
+    group_size = lax.axis_size("ep") // EXPERTS
+    slots = CAP // lax.axis_size("tp")
     normed = normalize(tokens, norm_gain)
     drive = jnp.dot(normed, w_in, preferred_element_type=jnp.float32).astype(jnp.bfloat16)
     activated, new_carried = state_update(
@@ -88,52 +86,49 @@
     partial_value = jnp.dot(activated, w_out, preferred_element_type=jnp.float32).astype(
         jnp.bfloat16
     )
-    summed = taken_together(partial_value.astype(jnp.float32).astype(jnp.bfloat16), "tp").astype(
-        jnp.float32
-    )
+    summed = partial_value.astype(jnp.float32) + swapped(partial_value).astype(jnp.float32)
     mixed = (tokens.astype(jnp.float32) + summed).astype(jnp.bfloat16)
     expert_in = normalize(mixed, expert_gain)
     weights = route_weights(route_logit)
-    ep_count = lax.axis_size("ep")
-    group_size = ep_count // EXPERTS
+    gate_both = jnp.concatenate([w_gate, swapped(w_gate)], axis=1)
+    up_both = jnp.concatenate([w_up, swapped(w_up)], axis=1)
+    down_both = jnp.concatenate([w_down, swapped(w_down)], axis=0)
     expert_ids = jnp.arange(EXPERTS, dtype=jnp.int32)
     routes_flat = route_ids.reshape(-1)
     weights_flat = weights.reshape(-1)
     onehot = (routes_flat[:, None] == expert_ids[None, :]).astype(jnp.int32)
     earlier = jnp.cumsum(onehot, axis=0) - onehot
-    slot_index = jnp.sum(earlier * onehot, axis=1)
-    position = routes_flat * CAP + slot_index
-    placement = (jnp.arange(EXPERTS * CAP, dtype=jnp.int32)[:, None] == position[None, :]).astype(
-        jnp.float32
-    )
-    per_token = placement.reshape(EXPERTS * CAP, count_rows, TOP).sum(axis=2)
+    slot_index = jnp.sum(earlier * onehot, axis=1) - core * slots
+    held = (slot_index >= 0) & (slot_index < slots)
+    position = jnp.where(held, routes_flat * slots + slot_index, -1)
+    placement = (
+        jnp.arange(EXPERTS * slots, dtype=jnp.int32)[:, None] == position[None, :]
+    ).astype(jnp.float32)
+    per_token = placement.reshape(EXPERTS * slots, count_rows, TOP).sum(axis=2)
     packed = jnp.dot(per_token.astype(jnp.bfloat16), expert_in, preferred_element_type=jnp.float32)
-    packed = packed.astype(jnp.bfloat16).reshape(EXPERTS, CAP, model_width)
+    packed = packed.astype(jnp.bfloat16).reshape(EXPERTS, slots, model_width)
     outgoing = jnp.repeat(packed, group_size, axis=0)
     received = lax.all_to_all(outgoing, "ep", split_axis=0, concat_axis=0, tiled=True)
-    sources, slots, features = received.shape
-    rows = received.reshape(sources * slots, features)
-    gated = jnp.dot(rows, w_gate, preferred_element_type=jnp.float32)
-    upward = jnp.dot(rows, w_up, preferred_element_type=jnp.float32)
+    rows = received.reshape(-1, model_width)
+    gated = jnp.dot(rows, gate_both, preferred_element_type=jnp.float32)
+    upward = jnp.dot(rows, up_both, preferred_element_type=jnp.float32)
     hidden = (jax.nn.silu(gated) * upward).astype(jnp.bfloat16)
-    produced = jnp.dot(hidden, w_down, preferred_element_type=jnp.float32)
-    produced = produced.reshape(sources, slots, features)
-    halves = lax.psum_scatter(
-        produced.astype(jnp.bfloat16), "tp", scatter_dimension=2, tiled=True
-    ).astype(jnp.float32)
-    returned = lax.all_to_all(
-        halves.astype(jnp.bfloat16), "ep", split_axis=0, concat_axis=0, tiled=True
-    ).astype(halves.dtype)
-    per_expert = returned.reshape(EXPERTS, group_size, CAP, -1).sum(axis=1)
-    per_expert = per_expert.reshape(EXPERTS * CAP, -1)
+    produced = jnp.dot(hidden, down_both, preferred_element_type=jnp.float32)
+    produced = produced.astype(jnp.bfloat16).reshape(received.shape)
+    returned = lax.all_to_all(produced, "ep", split_axis=0, concat_axis=0, tiled=True)
+    per_expert = returned.reshape(EXPERTS, group_size, slots, -1).astype(jnp.float32).sum(axis=1)
+    per_expert = per_expert.reshape(EXPERTS * slots, -1)
     weighing = (
-        (placement * weights_flat[None, :]).reshape(EXPERTS * CAP, count_rows, TOP).sum(axis=2)
+        (placement * weights_flat[None, :]).reshape(EXPERTS * slots, count_rows, TOP).sum(axis=2)
     )
     expert_sum = jnp.dot(weighing.T, per_expert, preferred_element_type=jnp.float32)
     half_width = model_width // lax.axis_size("tp")
-    column_start = lax.axis_index("tp") * half_width
-    own_mixed = lax.dynamic_slice_in_dim(mixed, column_start, half_width, 1)
-    new_tokens = (own_mixed.astype(jnp.float32) + expert_sum).astype(jnp.bfloat16)
+    own_sum = lax.dynamic_slice_in_dim(expert_sum, core * half_width, half_width, 1)
+    other_sum = lax.dynamic_slice_in_dim(expert_sum, (1 - core) * half_width, half_width, 1)
+    own_mixed = lax.dynamic_slice_in_dim(mixed, core * half_width, half_width, 1)
+    new_tokens = (own_mixed.astype(jnp.float32) + (own_sum + swapped(other_sum))).astype(
+        jnp.bfloat16
+    )
     return (new_tokens, new_carried)
 
 

time: 209 us -> 141 us (0.67)
  blocking collectives: 86.8 us -> 0 us
  waiting for transfers between devices: 54.1 us -> 83.4 us
  between operations: 14.3 us -> 0.94 us
  starting transfers between devices: 14.1 us -> 19 us
  local copies, waits for them, and re-layouts: 7.96 us -> 5.24 us
    all_to_all x1 -> x0, blocking collectives: 86.8 us -> none  [per_device(): lax.all_to_all(outgoing, 'ep', split_axis=0, concat_axis=0, tiled=True)]
    all_to_all x2, waiting for transfers between devices: 40.4 us -> 79.1 us  [the longest x1 41.7 us: per_device(): lax.all_to_all(produced, 'ep', split_axis=0, concat_axis=0, tiled=True)]
    reduce_scatter x1 -> x0, waiting for transfers between devices: 13.6 us -> none  [per_device(): lax.psum_scatter(produced.astype(jnp.bfloat16), 'tp', scatter_dimension=2...]
    ppermute x0 -> x5, waiting for transfers between devices: none -> 4.29 us  [swapped(): return lax.ppermute(shard, 'tp', [(0, 1), (1, 0)])]
    all_to_all x2, starting transfers between devices: 14.1 us -> 18.2 us  [the longest x1 11.5 us: per_device(): lax.all_to_all(outgoing, 'ep', split_axis=0, concat_axis=0, tiled=True)]
    unnamed x28 -> x24, local copies, waits for them, and re-layouts: 4.75 us -> 1.5 us
  transfers between devices with their start and end apart: 3 -> 7, of which waited for: 3 -> 4; matrix products, arithmetic and copies ran while one was open for 2% -> 7% of each run, Pallas kernels for 0% -> 0%
where the time goes in v1:
time: 141 us; the launch traced here: 140 us
  waiting for transfers between devices  83.4 us (59%)
  matrix products  23.9 us (17%)
  starting transfers between devices  19 us (13%)
  other arithmetic  7.09 us (5%)
  local copies, waits for them, and re-layouts  5.24 us (4%)
    all_to_all x1, waiting for transfers between devices, per_device(): lax.all_to_all(produced, 'ep', split_axis=0, concat_axis=0, tiled=True)  41.7 us
    all_to_all x1, waiting for transfers between devices, per_device(): lax.all_to_all(outgoing, 'ep', split_axis=0, concat_axis=0, tiled=True)  37.4 us
    all_to_all x1, starting transfers between devices, per_device(): lax.all_to_all(outgoing, 'ep', split_axis=0, concat_axis=0, tiled=True)  11.5 us
    dot_general x1, matrix products, per_device(): produced = jnp.dot(hidden, down_both, preferred_element_type=jnp.float32)  10.4 us
    all_to_all x1, starting transfers between devices, per_device(): lax.all_to_all(produced, 'ep', split_axis=0, concat_axis=0, tiled=True)  6.72 us
    dot_general x1, matrix products, per_device(): gated = jnp.dot(rows, gate_both, preferred_element_type=jnp.float32)  5.61 us
    ppermute x5, waiting for transfers between devices, swapped(): return lax.ppermute(shard, 'tp', [(0, 1), (1, 0)])  4.29 us
    dot_general x1, matrix products, per_device(): jnp.dot(normed, w_in, preferred_element_type=jnp.float32)  3.43 us
  transfers between devices with their start and end apart: 7, of which 4 were waited for; matrix products, arithmetic and copies ran while one was open for 7% of the time, Pallas kernels for 0%

profile of v1, /device:TPU:0, one launch (start us, length us, event | category | flops | bytes accessed | tf_op | source)
XLA Modules:
  0.0 139.5 jit_solution(5615736722293921061)
XLA Ops:
  0.6 0.0 copy-start
  0.7 0.7 exp.18
  1.4 1.1 fusion.35
  2.5 3.4 %convolution_convert_fusion.3 = bf16[32,768]{1,0:T(8,128)(2,1)S(1)} fusion(bf16[3072,768]{1,0:T(8,128)(2,1)} %param.26, bf16[32,3072]{1,0:T(8,128)(2,1)} %param.17, f32[3072]{0:T(1024)} %param.25, f32[32]{0:T(128)S(1)} %add_rsqrt_fusion.1), kind=kOutput, calls=%fused_computation.21 | convolution fusion | flops 151412736 | bytes 4976768 | tf_op jit(solution)/shard_map/dot_general | solution.py:82
  5.9 0.0 copy-start.5
  5.9 0.0 copy-start.6
  5.9 0.2 copy.39
  6.1 0.3 fusion.73
  6.4 0.3 convolution_bitcast_fusion
  6.8 0.2 cosine_multiply_fusion
  6.9 0.7 subtract_add_fusion
  7.7 0.0 copy-start.4
  7.7 1.6 %fusion.72 = (bf16[32,48,64]{2,0,1:T(8,128)(2,1)S(1)}, f32[32,48,64]{2,0,1:T(8,128)}) fusion(f32[32,48,128]{2,0,1:T(8,128)S(1)} %convolution_bitcast_fusion, f32[48,64]{1,0:T(8,128)S(1)} %get-tuple-element.18, f32[48,64]{1,0:T(8,128)S(1)} %get-tuple-element.19, f32[32,48,64]{2,1,0:T(8,128)S(1)} %get-tuple-element.15, f32[48,64]{1,0:T(8,128)S(1)} %get-tuple-element.17, ...), kind=kLoop, calls=%fused_computation.93 | loop fusion | flops 884736 | bytes 2211840 | tf_op jit(solution)/shard_map/neg | solution.py:45
  9.3 0.4 fusion.17
  9.7 0.0 copy-start.8
  9.8 0.1 copy.40
  9.9 0.0 copy-start.7
  9.9 3.2 %convolution_convert_fusion.2 = bf16[32,3072]{1,0:T(8,128)(2,1)S(1)} fusion(bf16[768,3072]{1,0:T(8,128)(2,1)} %param.27, f32[32,768]{1,0:T(8,128)S(1)} %copy.40, bf16[32,768]{1,0:T(8,128)(2,1)S(1)} %convolution_convert_fusion.3, f32[768]{0:T(1024)S(1)} %copy-done.9), kind=kOutput, calls=%fused_computation.16 | convolution fusion | flops 151388160 | bytes 5065728 | tf_op jit(solution)/shard_map/dot_general | solution.py:86
  13.1 0.0 collective-permute-start
  13.2 0.1 copy.41
  13.3 0.1 copy.43
  13.4 0.1 eq.31
  13.5 0.1 fusion.59
  13.6 0.1 reduce_window_sum.11
  13.7 0.2 select_reduce_fusion.1
  13.9 0.1 sub.47
  14.0 0.1 copy.44
  14.1 0.1 convert_reduce_fusion.1
  14.2 0.4 collective-permute-done
  14.6 0.2 fusion.32
  14.8 0.3 fusion.14
  15.2 2.0 %broadcast_in_dim.6 = bf16[8,8,8,3072]{3,2,1,0:T(8,128)(2,1)} broadcast(bf16[8,8,3072]{2,1,0:T(8,128)(2,1)S(1)} %fusion.14), dimensions={0,2,3} | broadcast | bytes 3538944 | tf_op jit(solution)/shard_map/broadcast_in_dim | solution.py:110
  17.2 11.5 %all-to-all-start = ((bf16[64,8,3072]{2,1,0:T(8,128)(2,1)}), bf16[64,8,3072]{2,1,0:T(8,128)(2,1)S(1)}, u32[]{:S(2)}, u32[]{:S(2)}) async-start(bf16[64,8,3072]{2,1,0:T(8,128)(2,1)} %bitcast.5), calls=%async_computation | async-start | bytes 6291456 | tf_op jit(solution)/shard_map/all_to_all | solution.py:111
  28.7 0.1 collective-permute-start.1
  28.8 0.5 collective-permute-start.2
  29.3 0.1 collective-permute-start.3
  29.4 3.8 %collective-permute-done.1 = bf16[3072,336]{0,1:T(8,128)(2,1)} collective-permute-done((bf16[3072,336]{0,1:T(8,128)(2,1)}, bf16[3072,336]{0,1:T(8,128)(2,1)}, u32[]{:S(2)}, u32[]{:S(2)}) %collective-permute-start.1) | collective-permute-done | bytes 2064416 | tf_op jit(solution)/shard_map/ppermute | solution.py:12
  33.3 37.4 %all-to-all-done = bf16[64,8,3072]{2,1,0:T(8,128)(2,1)S(1)} async-done(((bf16[64,8,3072]{2,1,0:T(8,128)(2,1)}), bf16[64,8,3072]{2,1,0:T(8,128)(2,1)S(1)}, u32[]{:S(2)}, u32[]{:S(2)}) %all-to-all-start) | async-done | bytes 3145760 | tf_op jit(solution)/shard_map/all_to_all | solution.py:111
  70.6 5.6 %fusion = f32[512,672]{0,1:T(8,128)} fusion(bf16[3072,336]{0,1:T(8,128)(2,1)} %collective-permute-done.1, bf16[3072,336]{0,1:T(8,128)(2,1)} %param.31, bf16[64,8,3072]{2,1,0:T(8,128)(2,1)S(1)} %all-to-all-done), kind=kOutput, calls=%fused_computation.2 | convolution fusion | flops 2122186752 | bytes 8650752 | tf_op jit(solution)/shard_map/dot_general | solution.py:113
  76.2 10.4 %fusion.11 = bf16[64,8,3072]{2,1,0:T(8,128)(2,1)} fusion(bf16[336,3072]{1,0:T(8,128)(2,1)} %collective-permute-done.3, bf16[336,3072]{1,0:T(8,128)(2,1)} %param.33, f32[512,672]{0,1:T(8,128)} %fusion, bf16[3072,336]{0,1:T(8,128)(2,1)} %collective-permute-done.2, bf16[3072,336]{0,1:T(8,128)(2,1)} %param.32, bf16[64,8,3072]{2,1,0:T(8,128)(2,1)S(1)} %all-to-all-done), kind=kOutput, calls=%fused_computation.13 | convolution fusion | flops 4248010752 | bytes 15925248 | tf_op jit(solution)/shard_map/dot_general | solution.py:116
  86.6 6.7 %all-to-all-start.1 = ((bf16[64,8,3072]{2,1,0:T(8,128)(2,1)}), bf16[64,8,3072]{2,1,0:T(8,128)(2,1)S(1)}, u32[]{:S(2)}, u32[]{:S(2)}) async-start(bf16[64,8,3072]{2,1,0:T(8,128)(2,1)} %fusion.11), calls=%async_computation.1 | async-start | bytes 6291456 | tf_op jit(solution)/shard_map/all_to_all | solution.py:118
  93.4 41.7 %all-to-all-done.1 = bf16[64,8,3072]{2,1,0:T(8,128)(2,1)S(1)} async-done(((bf16[64,8,3072]{2,1,0:T(8,128)(2,1)}), bf16[64,8,3072]{2,1,0:T(8,128)(2,1)S(1)}, u32[]{:S(2)}, u32[]{:S(2)}) %all-to-all-start.1) | async-done | bytes 3145760 | tf_op jit(solution)/shard_map/all_to_all | solution.py:118
  135.1 0.5 convert_reduce_fusion
  135.6 0.2 fusion.20
  135.8 0.1 collective-permute-start.4
  135.9 1.6 %pad_maximum_fusion = f32[32,48,128]{2,0,1:T(8,128)S(1)} fusion(f32[32,48,64]{2,0,1:T(8,128)} %get-tuple-element.13, f32[32,48,64]{2,0,1:T(8,128)} %copy-done.1), kind=kLoop, calls=%fused_computation.25 | loop fusion | flops 196608 | bytes 1572864 | tf_op jit(solution)/shard_map/concatenate | solution.py:49
  137.5 1.3 copy.45
  138.9 0.7 add_convert_fusion
  (27 shorter events, 0.1 us)
Async XLA Ops:
  0.6 5.8 %copy-start = (bf16[48,128,16]{1,2,0:T(8,128)(2,1)S(1)}, bf16[48,128,16]{1,2,0:T(8,128)(2,1)}, u32[]{:S(2)}) copy-start(bf16[48,128,16]{1,2,0:T(8,128)(2,1)} %param.22) | copy-start | bytes 589828
  0.6 5.5 %copy-start.2 = (f32[32,48,128]{2,1,0:T(8,128)S(1)}, f32[32,48,128]{2,1,0:T(8,128)}, u32[]{:S(2)}) copy-start(f32[32,48,128]{2,1,0:T(8,128)} %param.18) | copy-start | bytes 2359300
  5.9 0.8 copy-start.5
  5.9 0.8 copy-start.6
  7.7 1.7 %copy-start.1 = (f32[32,48,64]{2,0,1:T(8,128)}, f32[32,48,64]{2,0,1:T(8,128)S(1)}, u32[]{:S(2)}) copy-start(f32[32,48,64]{2,0,1:T(8,128)S(1)} %subtract_add_fusion) | copy-start | bytes 1179652
  7.7 1.7 %copy-start.4 = (bf16[48,16,128]{2,1,0:T(8,128)(2,1)S(1)}, bf16[48,16,128]{2,1,0:T(8,128)(2,1)}, u32[]{:S(2)}) copy-start(bf16[48,16,128]{2,1,0:T(8,128)(2,1)} %param.23) | copy-start | bytes 589828
  7.7 2.2 %copy-start.9 = (f32[768]{0:T(1024)S(1)}, f32[768]{0:T(1024)}, u32[]{:S(2)}) copy-start(f32[768]{0:T(1024)} %param.24) | copy-start | bytes 9220
  9.7 3.4 %copy-start.8 = (s32[32,2]{0,1:T(2,128)S(1)}, s32[32,2]{0,1:T(2,128)}, u32[]{:S(2)}) copy-start(s32[32,2]{0,1:T(2,128)} %param.29) | copy-start | bytes 772
  9.7 3.5 %copy-start.10 = (f32[32,2]{0,1:T(2,128)S(1)}, f32[32,2]{0,1:T(2,128)}, u32[]{:S(2)}) copy-start(f32[32,2]{0,1:T(2,128)} %param.30) | copy-start | bytes 772
  9.8 4.9 %copy-start.3 = (bf16[32,3072]{1,0:T(8,128)(2,1)S(1)}, bf16[32,3072]{1,0:T(8,128)(2,1)}, u32[]{:S(2)}) copy-start(bf16[32,3072]{1,0:T(8,128)(2,1)} %param.17) | copy-start | bytes 589828
  9.9 4.9 %copy-start.7 = (f32[3072]{0:T(1024)S(1)}, f32[3072]{0:T(1024)}, u32[]{:S(2)}) copy-start(f32[3072]{0:T(1024)} %param.28) | copy-start | bytes 36868
  13.1 1.5 %collective-permute-start = (bf16[32,3072]{1,0:T(8,128)(2,1)S(1)}, bf16[32,3072]{1,0:T(8,128)(2,1)S(1)}, u32[]{:S(2)}, u32[]{:S(2)}) collective-permute-start(bf16[32,3072]{1,0:T(8,128)(2,1)S(1)} %convolution_convert_fusion.2), channel_id=1, source_target_pairs={{0,1},{1,0},{2,3},{3,2},{4,5},{5,4},{6,7},{7,6},{8,9},{9,8},{10,11... | collective-permute-start | bytes 589832 | tf_op jit(solution)/shard_map/ppermute | solution.py:12
  17.2 53.4 %all-to-all-start = ((bf16[64,8,3072]{2,1,0:T(8,128)(2,1)}), bf16[64,8,3072]{2,1,0:T(8,128)(2,1)S(1)}, u32[]{:S(2)}, u32[]{:S(2)}) async-start(bf16[64,8,3072]{2,1,0:T(8,128)(2,1)} %bitcast.5), calls=%async_computation | async-start | bytes 6291456 | tf_op jit(solution)/shard_map/all_to_all | solution.py:111
  28.7 4.5 %collective-permute-start.1 = (bf16[3072,336]{0,1:T(8,128)(2,1)}, bf16[3072,336]{0,1:T(8,128)(2,1)}, u32[]{:S(2)}, u32[]{:S(2)}) collective-permute-start(bf16[3072,336]{0,1:T(8,128)(2,1)} %param.31), channel_id=1, source_target_pairs={{0,1},{1,0},{2,3},{3,2},{4,5},{5,4},{6,7},{7,6},{8,9},{9,8},{10,11... | collective-permute-start | bytes 6193160 | tf_op jit(solution)/shard_map/ppermute | solution.py:12
  28.8 47.4 %collective-permute-start.2 = (bf16[3072,336]{0,1:T(8,128)(2,1)}, bf16[3072,336]{0,1:T(8,128)(2,1)}, u32[]{:S(2)}, u32[]{:S(2)}) collective-permute-start(bf16[3072,336]{0,1:T(8,128)(2,1)} %param.32), channel_id=1, source_target_pairs={{0,1},{1,0},{2,3},{3,2},{4,5},{5,4},{6,7},{7,6},{8,9},{9,8},{10,11... | collective-permute-start | bytes 6193160 | tf_op jit(solution)/shard_map/ppermute | solution.py:12
  29.3 46.9 %collective-permute-start.3 = (bf16[336,3072]{1,0:T(8,128)(2,1)}, bf16[336,3072]{1,0:T(8,128)(2,1)}, u32[]{:S(2)}, u32[]{:S(2)}) collective-permute-start(bf16[336,3072]{1,0:T(8,128)(2,1)} %param.33), channel_id=1, source_target_pairs={{0,1},{1,0},{2,3},{3,2},{4,5},{5,4},{6,7},{7,6},{8,9},{9,8},{10,11... | collective-permute-start | bytes 6193160 | tf_op jit(solution)/shard_map/ppermute | solution.py:12
  86.6 48.4 %all-to-all-start.1 = ((bf16[64,8,3072]{2,1,0:T(8,128)(2,1)}), bf16[64,8,3072]{2,1,0:T(8,128)(2,1)S(1)}, u32[]{:S(2)}, u32[]{:S(2)}) async-start(bf16[64,8,3072]{2,1,0:T(8,128)(2,1)} %fusion.11), calls=%async_computation.1 | async-start | bytes 6291456 | tf_op jit(solution)/shard_map/all_to_all | solution.py:118
  135.8 3.1 %collective-permute-start.4 = (f32[32,1536]{1,0:T(8,128)S(1)}, f32[32,1536]{1,0:T(8,128)S(1)}, u32[]{:S(2)}, u32[]{:S(2)}) collective-permute-start(f32[32,1536]{1,0:T(8,128)S(1)} %constant_dynamic-slice_fusion), channel_id=1, source_target_pairs={{0,1},{1,0},{2,3},{3,2},{4,5},{5,4},{6,7},{7,6},{8,9},{9,8},{10,11... | collective-permute-start | bytes 589832 | tf_op jit(solution)/shard_map/ppermute | solution.py:12
